TPU v7x, 32 devices: a whole 2x2x4 slice. The times are simulated.
32 devices in a mesh: ep: 8 (over z, core), tp: 4 (over y, x).
Axes of the slice: x: 2, y: 2, z: 4, core: 2. Of those that a mesh axis runs over, the one named last changes fastest.
Arguments:
- token_rows: bfloat16 [192, 2048], P('ep', 'tp'), may hold values from -6 to 6
- prior_state: float32 [192, 64, 2048], P('ep', None, 'tp'), may hold values from -4 to 4
- first_gain: bfloat16 [2048], replicated, may hold values from 0.099609375 to 1.8984375
- w_recept: bfloat16 [2048, 2048], P(None, 'tp'), may hold values from -0.125 to 0.125
- w_key: bfloat16 [2048, 2048], P(None, 'tp'), may hold values from -0.125 to 0.125
- w_value: bfloat16 [2048, 2048], P(None, 'tp'), may hold values from -0.125 to 0.125
- decay_down: bfloat16 [2048, 96], P('tp'), may hold values from -0.125 to 0.125
- decay_up: bfloat16 [96, 2048], P(None, 'tp'), may hold values from -0.625 to 0.625
- decay_base: float32 [2048], P('tp'), may hold values from -4 to 3
- iclr_down: bfloat16 [2048, 96], P('tp'), may hold values from -0.125 to 0.125
- iclr_up: bfloat16 [96, 2048], P(None, 'tp'), may hold values from -0.625 to 0.625
- iclr_base: float32 [2048], P('tp'), may hold values from -4 to 4
- key_scale: bfloat16 [2048], P('tp'), may hold values from 0.29882812 to 1.5
- key_mix: bfloat16 [2048], P('tp'), may hold values from 0 to 2
- head_gain: bfloat16 [2048], P('tp'), may hold values from 0.099609375 to 1.8984375
- w_out: bfloat16 [2048, 2048], P(None, 'tp'), may hold values from -0.125 to 0.125
- second_gain: bfloat16 [2048], replicated, may hold values from 0.099609375 to 1.8984375
- routes: int32 [192, 4], P('ep'), may hold values from 0 to 7, all different within a row; in each aligned block of 24 rows (0 to 23, 24 to 47, ...) at most 18 rows name the same one
- route_weights: float32 [192, 4], P('ep'), may hold values from 0.2 to 1
- exp_gate: bfloat16 [8, 2048, 2048], P('ep', None, 'tp'), may hold values from -0.125 to 0.125
- exp_up: bfloat16 [8, 2048, 2048], P('ep', None, 'tp'), may hold values from -0.125 to 0.125
- exp_down: bfloat16 [8, 2048, 2048], P('ep', 'tp'), may hold values from -0.125 to 0.125
- dense_gate: bfloat16 [2048, 512], P(None, 'tp'), may hold values from -0.125 to 0.125
- dense_up: bfloat16 [2048, 512], P(None, 'tp'), may hold values from -0.125 to 0.125
- dense_down: bfloat16 [512, 2048], P('tp'), may hold values from -0.25 to 0.25
- dense_mix: bfloat16 [2048], replicated, may hold values from -0.125 to 0.125
Outputs:
- layer_out: bfloat16 [192, 2048], P('ep', 'tp')
- next_state: float32 [192, 64, 2048], P('ep', None, 'tp')
Inputs may be any that keep to these rules, and one draw needn't show every extreme that they name: `routes`: each row names 4 different experts. Among the rows of one index of ep no expert is named by more than 18 rows, and in every draw some expert is named by exactly 18 of them.
All inputs are finite; a program needn't handle non-finite values.
Results may differ from a plain program's by a relative error of at most 0.018.
Values may be sent and summed in bfloat16 or wider, within the bound.
A program may use at most 64 MiB of HBM per device.

v0:
```python
import jax
import jax.numpy as jnp
from jax import lax
from jax.sharding import PartitionSpec as P

HEAD = 64


norm_eps = 1e-06
head_eps = 0.00064
key_eps = 1e-06


def product(left, right):
    return jnp.dot(left, right, preferred_element_type=jnp.float32)


def scale_rows(values, mean_square, gain):
    return (values * lax.rsqrt(mean_square + norm_eps) * gain.astype(jnp.float32)).astype(
        jnp.bfloat16
    )


def first_norm_rows(token_rows, gain):
    own_width = token_rows.shape[1]
    start = lax.axis_index("tp") * own_width
    gathered = lax.all_gather(token_rows, "tp", axis=1, tiled=True)
    values = gathered.astype(jnp.float32)
    full_rows = scale_rows(values, jnp.mean(values * values, axis=1, keepdims=True), gain)
    own_cols = lax.dynamic_slice_in_dim(full_rows, start, own_width, 1)
    return (full_rows, own_cols)


def second_norm_rows(residual, gain):
    own_width = residual.shape[1]
    start = lax.axis_index("tp") * own_width
    gathered = lax.all_gather(residual, "tp", axis=1, tiled=True)
    values = gathered.astype(jnp.float32)
    full_rows = scale_rows(values, jnp.mean(values * values, axis=1, keepdims=True), gain)
    own_cols = lax.dynamic_slice_in_dim(full_rows, start, own_width, 1)
    return (full_rows, own_cols)


def local(
    token_rows,
    prior_state,
    first_gain,
    w_recept,
    w_key,
    w_value,
    decay_down,
    decay_up,
    decay_base,
    iclr_down,
    iclr_up,
    iclr_base,
    key_scale,
    key_mix,
    head_gain,
    w_out,
    second_gain,
    routes,
    route_weights,
    exp_gate,
    exp_up,
    exp_down,
    dense_gate,
    dense_up,
    dense_down,
    dense_mix,
):
    seq_count, own_width = token_rows.shape
    heads_dev = own_width // HEAD
    first_full, first_own = first_norm_rows(token_rows, first_gain)
    decay_low, rate_low = lax.psum(
        (product(first_own, decay_down), product(first_own, iclr_down)), "tp"
    )
    decay_act = jnp.tanh(decay_low).astype(jnp.bfloat16)
    rate_act = rate_low.astype(jnp.bfloat16)
    recept = product(first_full, w_recept).astype(jnp.bfloat16)
    key_rows = product(first_full, w_key).astype(jnp.bfloat16)
    value_rows = product(first_full, w_value).astype(jnp.bfloat16)
    decay_rate = jnp.exp(
        -jnp.exp(-jax.nn.softplus(-(decay_base + product(decay_act, decay_up))) - 0.5)
    )
    iclr_rate = jax.nn.sigmoid(iclr_base + product(rate_act, iclr_up))
    key_float = key_rows.astype(jnp.float32)
    scaled = (key_float * key_scale.astype(jnp.float32)).reshape(seq_count, heads_dev, HEAD)
    removal = scaled * lax.rsqrt(jnp.sum(scaled * scaled, axis=-1, keepdims=True) + key_eps)
    written = (key_float * (1.0 + (iclr_rate - 1.0) * key_mix.astype(jnp.float32))).reshape(
        seq_count, heads_dev, HEAD
    )
    state_grid = prior_state.reshape(seq_count, HEAD, heads_dev, HEAD)
    recall = jnp.sum(state_grid * removal[:, None], axis=-1)
    scaled_removal = removal * iclr_rate.reshape(seq_count, heads_dev, HEAD)
    value_cols = jnp.transpose(
        value_rows.astype(jnp.float32).reshape(seq_count, heads_dev, HEAD), (0, 2, 1)
    )
    state_grid = (
        state_grid * decay_rate.reshape(seq_count, 1, heads_dev, HEAD)
        - recall[..., None] * scaled_removal[:, None]
        + value_cols[..., None] * written[:, None]
    )
    read = jnp.sum(
        state_grid * recept.astype(jnp.float32).reshape(seq_count, 1, heads_dev, HEAD), axis=-1
    )
    read = jnp.transpose(read, (0, 2, 1))
    centered = read - jnp.mean(read, axis=-1, keepdims=True)
    variance = jnp.mean(centered * centered, axis=-1, keepdims=True)
    head_out = (
        centered
        * lax.rsqrt(variance + head_eps)
        * head_gain.astype(jnp.float32).reshape(heads_dev, HEAD)
    )
    head_out = head_out.reshape(seq_count, own_width).astype(jnp.bfloat16)
    heads_all = lax.all_gather(head_out, "tp", axis=1, tiled=True)
    mixer_out = product(heads_all, w_out).astype(jnp.bfloat16)
    residual = (token_rows.astype(jnp.float32) + mixer_out.astype(jnp.float32)).astype(jnp.bfloat16)
    second_full, second_own = second_norm_rows(residual, second_gain)
    dense_hidden = (
        jax.nn.silu(product(second_full, dense_gate)) * product(second_full, dense_up)
    ).astype(jnp.bfloat16)
    dense_out = lax.psum_scatter(
        product(dense_hidden, dense_down).astype(jnp.bfloat16),
        "tp",
        scatter_dimension=1,
        tiled=True,
    ).astype(jnp.float32)
    mix_gate = jax.nn.sigmoid(product(second_full, dense_mix[:, None])[:, 0])
    group_count = lax.axis_size("ep")
    local_experts = exp_gate.shape[0]
    experts = local_experts * group_count
    top_count = routes.shape[1]
    capacity = max(2, 3 * seq_count * top_count // (2 * experts))
    assign_count = seq_count * top_count
    flat_ids = routes.reshape(assign_count)
    onehot = (flat_ids[:, None] == jnp.arange(experts, dtype=jnp.int32)[None, :]).astype(
        jnp.float32
    )
    earlier = (jnp.arange(assign_count)[:, None] > jnp.arange(assign_count)[None, :]).astype(
        jnp.float32
    )
    before = jnp.dot(earlier, onehot, precision=lax.Precision.HIGHEST)
    ranking = jnp.sum(before * onehot, axis=1).astype(jnp.int32)
    slot_index = flat_ids * capacity + ranking
    slot_total = experts * capacity
    slot_onehot = (jnp.arange(slot_total, dtype=jnp.int32)[:, None] == slot_index[None, :]).astype(
        jnp.bfloat16
    )
    repeated = jnp.repeat(second_full, top_count, axis=0)
    outgoing = product(slot_onehot, repeated).astype(jnp.bfloat16)
    outgoing = outgoing.reshape(group_count, local_experts, capacity, second_full.shape[1])
    arrived = lax.all_to_all(outgoing, "ep", split_axis=0, concat_axis=0, tiled=True)
    gate_act = jnp.einsum("secd,edf->secf", arrived, exp_gate, preferred_element_type=jnp.float32)
    up_act = jnp.einsum("secd,edf->secf", arrived, exp_up, preferred_element_type=jnp.float32)
    hidden = (jax.nn.silu(gate_act) * up_act).astype(jnp.bfloat16)
    partial_value = jnp.einsum(
        "secf,efd->secd", hidden, exp_down, preferred_element_type=jnp.float32
    ).astype(jnp.bfloat16)
    partial_value = lax.optimization_barrier(partial_value)
    summed = lax.psum_scatter(
        partial_value.astype(jnp.float32).astype(jnp.bfloat16),
        "tp",
        scatter_dimension=3,
        tiled=True,
    )
    returned = lax.all_to_all(summed, "ep", split_axis=0, concat_axis=0, tiled=True)
    returned = returned.reshape(slot_total, own_width)
    picked = jnp.take(returned, slot_index, axis=0).astype(jnp.float32)
    weighted = picked * route_weights.reshape(assign_count)[:, None]
    routed = jnp.sum(weighted.reshape(seq_count, top_count, own_width), axis=1)
    layer_out = residual.astype(jnp.float32) + routed + mix_gate[:, None] * dense_out
    return (layer_out.astype(jnp.bfloat16), state_grid.reshape(seq_count, HEAD, own_width))


def solution(mesh):
    in_specs = (
        P("ep", "tp"),
        P("ep", None, "tp"),
        P(),
        P(None, "tp"),
        P(None, "tp"),
        P(None, "tp"),
        P("tp", None),
        P(None, "tp"),
        P("tp"),
        P("tp", None),
        P(None, "tp"),
        P("tp"),
        P("tp"),
        P("tp"),
        P("tp"),
        P(None, "tp"),
        P(),
        P("ep", None),
        P("ep", None),
        P("ep", None, "tp"),
        P("ep", None, "tp"),
        P("ep", "tp", None),
        P(None, "tp"),
        P(None, "tp"),
        P("tp", None),
        P(),
    )
    out_specs = (P("ep", "tp"), P("ep", None, "tp"))
    return jax.shard_map(local, mesh=mesh, in_specs=in_specs, out_specs=out_specs, check_vma=False)
```

profile of v0, /device:TPU:0, one launch (start us, length us, event | category | flops | bytes accessed | tf_op | source)
XLA Modules:
  0.0 181.4 jit_solution(9681087698319180133)
XLA Ops:
  7.2 0.8 convert_element_type.135
  8.1 0.7 convert_element_type.138
  8.7 0.8 reshape.209
  9.5 0.7 convert_element_type.130
  10.2 1.3 convert_element_type.149
  11.5 0.8 copy.47
  12.3 0.1 fusion.33
  12.5 0.6 multiply_add_fusion.1
  13.2 10.0 %all_gather.9 = bf16[24,2048]{1,0:T(8,128)(2,1)S(1)} all-gather(bf16[24,512]{1,0:T(8,128)(2,1)} %param.26), channel_id=1, replica_groups=mesh['ep'=8,'tp'=4] {'tp'}, dimensions={1}, use_global_device_ids=true | all-gather | bytes 122880 | tf_op jit(solution)/shard_map/all_gather | solution.py:27
  23.2 0.1 fusion.49
  23.3 0.1 fusion.51
  23.4 1.0 fusion.62
  24.5 1.0 fusion.64
  25.5 2.0 %fusion.29 = f32[24,512]{1,0:T(8,128)S(1)} fusion(bf16[24,2048]{1,0:T(8,128)(2,1)S(1)} %fusion.51, bf16[2048,512]{1,0:T(8,128)(2,1)} %param.29), kind=kOutput, calls=%fused_computation.30 | convolution fusion | flops 50356224 | bytes 2244608 | tf_op jit(solution)/shard_map/dot_general | solution.py:15
  27.6 2.0 %fusion.30 = f32[24,512]{1,0:T(8,128)S(1)} fusion(bf16[24,2048]{1,0:T(8,128)(2,1)S(1)} %fusion.51, bf16[2048,512]{1,0:T(8,128)(2,1)} %param.31), kind=kOutput, calls=%fused_computation.32 | convolution fusion | flops 50356224 | bytes 2244608 | tf_op jit(solution)/shard_map/dot_general | solution.py:15
  29.7 2.0 %broadcast_multiply_fusion.1 = (f32[24,512]{1,0:T(8,128)S(1)}, f32[24,512]{1,0:T(8,128)S(1)}) fusion(f32[512]{0:T(512)S(1)} %convert_element_type.135, bf16[24,2048]{1,0:T(8,128)(2,1)S(1)} %fusion.51, bf16[2048,512]{1,0:T(8,128)(2,1)} %param.30), kind=kOutput, calls=%fused_computation.81 | convolution fusion | flops 50368512 | bytes 2295808 | tf_op jit(solution)/shard_map/dot_general | solution.py:15
  31.8 0.1 multiply_reduce_fusion.4
  32.1 15.2 %all-reduce = (bf16[24,96]{1,0:T(8,128)(2,1)S(1)}, f32[24,96]{1,0:T(8,128)S(1)}) all-reduce(f32[24,96]{1,0:T(8,128)S(1)} %fusion.62, f32[24,96]{1,0:T(8,128)S(1)} %fusion.64), channel_id=1, replica_groups=mesh['ep'=8,'tp'=4] {'tp'}, use_global_device_ids=true, to_apply=%region_4.5 | all-reduce | flops 4608 | bytes 32256 | tf_op jit(solution)/shard_map/psum | solution.py:75
  47.3 0.8 multiply_multiply_fusion
  48.4 0.2 fusion.60
  48.7 0.5 copy-done.10
  49.2 0.3 copy.44
  49.5 5.6 %reshape.195 = f32[24,64,8,64]{3,2,1,0:T(8,128)} reshape(f32[24,64,512]{2,1,0:T(8,128)} %param.27) | data formatting | bytes 6291456 | tf_op jit(solution)/shard_map/reshape | solution.py:93
  55.1 4.7 %multiply_reduce_fusion.1 = f32[24,64,8]{2,1,0:T(8,128)S(1)} fusion(f32[24,64,8,64]{3,2,1,0:T(8,128)} %reshape.195, f32[24,8,64]{2,1,0:T(8,128)S(1)} %get-tuple-element.5), kind=kLoop, calls=%fused_computation.2 | loop fusion | flops 1560576 | bytes 3244032 | tf_op jit(solution)/shard_map/reduce_sum | solution.py:94
  59.8 5.8 %multiply_reduce_fusion = f32[24,64,8]{2,1,0:T(8,128)S(1)} fusion(f32[24,64,8,64]{3,2,1,0:T(8,128)S(1)} %copy-done.1, f32[24,8,64]{2,1,0:T(8,128)S(1)} %reshape.208, f32[24,8,64]{2,1,0:T(8,128)S(1)} %mul.280, f32[24,64,8]{2,1,0:T(8,128)S(1)} %copy.44, f32[24,8,64]{2,1,0:T(8,128)S(1)} %get-tuple-element.4, f32[24,64,8]{2,1,0:T(8,128)S(1)} %multiply_reduce_fusion.1, ...), kind=kLoop, calls=%fused_computation.1 | loop fusion | flops 5492736 | bytes 3489792 | tf_op jit(solution)/shard_map/reduce_sum | solution.py:104
  65.7 0.1 multiply_reduce_fusion.2
  65.8 0.1 multiply_convert_fusion
  66.0 0.2 copy.46
  66.1 0.1 convert_element_type.141
  66.3 8.4 %all_gather.10 = bf16[24,2048]{1,0:T(8,128)(2,1)S(1)} all-gather(bf16[24,512]{1,0:T(8,128)(2,1)S(1)} %convert_element_type.141), channel_id=1, replica_groups=mesh['ep'=8,'tp'=4] {'tp'}, dimensions={1}, use_global_device_ids=true | all-gather | bytes 122880 | tf_op jit(solution)/shard_map/all_gather | solution.py:116
  74.7 2.0 %fusion.28 = bf16[24,512]{1,0:T(8,128)(2,1)S(1)} fusion(bf16[24,2048]{1,0:T(8,128)(2,1)S(1)} %all_gather.10, bf16[2048,512]{1,0:T(8,128)(2,1)} %param.41, bf16[24,512]{1,0:T(8,128)(2,1)S(1)} %copy-done.12), kind=kOutput, calls=%fused_computation.28 | convolution fusion | flops 50393088 | bytes 2244608 | tf_op jit(solution)/shard_map/dot_general | solution.py:15
  76.6 7.3 %all_gather.11 = bf16[24,2048]{1,0:T(8,128)(2,1)S(1)} all-gather(bf16[24,512]{1,0:T(8,128)(2,1)S(1)} %fusion.28), channel_id=1, replica_groups=mesh['ep'=8,'tp'=4] {'tp'}, dimensions={1}, use_global_device_ids=true | all-gather | bytes 122880 | tf_op jit(solution)/shard_map/all_gather | solution.py:37
  84.0 0.1 fusion.52
  84.2 0.6 copy-done.4
  84.8 0.2 broadcast_in_dim.10
  85.0 0.8 reshape.200
  85.9 1.3 convolution_convert_fusion.1
  87.2 1.1 reshape.201
  88.2 25.8 %all_to_all.10 = bf16[8,1,18,2048]{3,2,1,0:T(8,128)(2,1)S(1)} all-to-all(bf16[8,1,18,2048]{3,2,1,0:T(8,128)(2,1)} %bitcast.112), channel_id=1, replica_groups=mesh['ep'=8,'tp'=4] {'ep'}, dimensions={0} | all-to-all | bytes 1179648 | tf_op jit(solution)/shard_map/all_to_all | solution.py:153
  114.0 0.9 copy-done.3
  114.9 2.9 %fusion.6 = f32[8,1,18,512]{3,2,0,1:T(8,128)} fusion(bf16[1,2048,512]{2,1,0:T(8,128)(2,1)} %param.45, bf16[8,1,18,2048]{3,2,1,0:T(8,128)(2,1)S(1)} %all_to_all.10), kind=kOutput, calls=%fused_computation.13 | convolution fusion | flops 301989888 | bytes 2981888 | tf_op jit(solution)/shard_map/secd,edf->secf/dot_general | solution.py:154
  117.9 3.9 %fusion = bf16[8,1,18,2048]{3,2,0,1:T(8,128)(2,1)} fusion(bf16[1,512,2048]{2,1,0:T(8,128)(2,1)S(1)} %copy-done, bf16[1,2048,512]{2,1,0:T(8,128)(2,1)} %param.46, bf16[8,1,18,2048]{3,2,1,0:T(8,128)(2,1)} %copy-done.3, f32[8,1,18,512]{3,2,0,1:T(8,128)} %fusion.6), kind=kOutput, calls=%fused_computation.6 | convolution fusion | flops 604717056 | bytes 5668864 | tf_op jit(solution)/shard_map/secf,efd->secd/dot_general | solution.py:157
  121.8 0.2 reduce-scatter.5.cloned.1.call-start
  122.1 0.8 fusion.80
  122.9 2.2 %convolution_convert_fusion.2 = bf16[24,2048]{1,0:T(8,128)(2,1)} fusion(bf16[128,2048]{1,0:T(8,128)(2,1)} %param.50, bf16[24,2048]{1,0:T(8,128)(2,1)S(1)} %copy-done.5, bf16[2048,128]{1,0:T(8,128)(2,1)} %param.49, f32[24,128]{1,0:T(8,128)} %fusion.80), kind=kOutput, calls=%fused_computation.7 | convolution fusion | flops 25233408 | bytes 1257472 | tf_op jit(solution)/shard_map/dot_general | solution.py:15
  125.1 0.7 broadcast_multiply_fusion.3
  125.8 0.6 convert_element_type.146
  126.4 0.7 reshape.222
  127.1 0.1 mul.306
  127.2 0.8 copy.53
  128.2 0.7 compare_and_fusion
  128.9 0.1 copy.49
  129.0 0.1 fusion.37
  129.1 5.3 %mul.272 = f32[24,64,8,64]{3,2,1,0:T(8,128)} broadcast(f32[24,64,8]{2,1,0:T(8,128)} %copy-done.2), dimensions={0,1,2} | broadcast | bytes 3194880 | tf_op jit(solution)/shard_map/mul | solution.py:101
  134.4 6.3 %mul.315 = f32[24,64,512]{2,1,0:T(8,128)} reshape(f32[24,64,8,64]{3,2,1,0:T(8,128)} %mul.272) | data formatting | bytes 6291456 | tf_op jit(solution)/shard_map/mul | solution.py:101
  140.7 3.8 %mul.276 = f32[24,64,8,64]{3,2,1,0:T(8,128)} broadcast(f32[24,64,8]{2,1,0:T(8,128)S(1)} %copy.44), dimensions={0,1,2} | broadcast | bytes 3194880 | tf_op jit(solution)/shard_map/mul | solution.py:102
  144.5 6.3 %mul.321 = f32[24,64,512]{2,1,0:T(8,128)} reshape(f32[24,64,8,64]{3,2,1,0:T(8,128)} %mul.276) | data formatting | bytes 6291456 | tf_op jit(solution)/shard_map/mul | solution.py:102
  150.8 7.0 %multiply_add_fusion = f32[24,64,512]{2,1,0:T(8,128)} fusion(f32[24,64,512]{2,1,0:T(8,128)} %mul.321, f32[24,64,512]{2,1,0:T(8,128)} %mul.315, f32[24,64,512]{2,1,0:T(8,128)} %param.27, f32[24,512]{1,0:T(8,128)S(1)} %get-tuple-element.7, f32[24,512]{1,0:T(8,128)S(1)} %copy-done.9, f32[24,512]{1,0:T(8,128)S(1)} %copy-done.11), kind=kLoop, calls=%fused_computation.3 | loop fusion | flops 3932160 | bytes 12730368 | tf_op jit(solution)/shard_map/add | solution.py:100
  157.8 3.4 %all-to-all-start.1 = ((bf16[8,1,18,512]{3,2,1,0:T(8,128)(2,1)}), bf16[8,1,18,512]{3,2,1,0:T(8,128)(2,1)S(1)}, u32[]{:S(2)}, u32[]{:S(2)}) async-start(bf16[8,1,18,512]{3,2,1,0:T(8,128)(2,1)} %bitcast.114), calls=%async_computation.2 | async-start | bytes 393216 | tf_op jit(solution)/shard_map/all_to_all | solution.py:167
  161.2 8.2 %all-to-all-done.1 = bf16[8,1,18,512]{3,2,1,0:T(8,128)(2,1)S(1)} async-done(((bf16[8,1,18,512]{3,2,1,0:T(8,128)(2,1)}), bf16[8,1,18,512]{3,2,1,0:T(8,128)(2,1)S(1)}, u32[]{:S(2)}, u32[]{:S(2)}) %all-to-all-start.1) | async-done | bytes 147488 | tf_op jit(solution)/shard_map/all_to_all | solution.py:167
  169.5 0.8 gather_fusion
  170.3 0.2 multiply_reduce_fusion.3
  170.5 2.6 %reduce-scatter.5.cloned.1.call-done = bf16[24,512]{1,0:T(8,128)(2,1)} async-done(((bf16[24,2048]{1,0:T(8,128)(2,1)}), bf16[24,512]{1,0:T(8,128)(2,1)}) %reduce-scatter.5.cloned.1.call-update) | async-done | bytes 24592 | tf_op jit(solution)/shard_map/reduce_scatter | solution.py:123
  173.1 1.4 add_convert_fusion
  (66 shorter events, 1.7 us)
Async XLA Ops:
  7.2 110.7 %copy-start = (bf16[1,512,2048]{2,1,0:T(8,128)(2,1)S(1)}, bf16[1,512,2048]{2,1,0:T(8,128)(2,1)}, u32[]{:S(2)}) copy-start(bf16[1,512,2048]{2,1,0:T(8,128)(2,1)} %param.47) | copy-start | bytes 6291460
  7.2 150.6 %reduce-scatter.3.cloned.1.call-start = ((), (), s32[]{:S(2)}) async-start(), calls=%async_computation.4 | async-start | bytes 983040 | tf_op jit(solution)/shard_map/reduce_scatter | solution.py:161
  12.5 19.2 %copy-start.18 = (f32[96]{0:T(128)}, f32[96]{0:T(128)S(1)}, u32[]{:S(2)}) copy-start(f32[96]{0:T(128)S(1)} %fusion.33) | copy-start | bytes 1156
  27.5 19.9 %copy-start.13 = (bf16[96,512]{1,0:T(8,128)(2,1)S(1)}, bf16[96,512]{1,0:T(8,128)(2,1)}, u32[]{:S(2)}) copy-start(bf16[96,512]{1,0:T(8,128)(2,1)} %param.36) | copy-start | bytes 294916
  27.5 19.9 %copy-start.15 = (f32[512]{0:T(512)S(1)}, f32[512]{0:T(512)}, u32[]{:S(2)}) copy-start(f32[512]{0:T(512)} %param.37) | copy-start | bytes 6148
  27.6 20.8 %copy-start.16 = (bf16[96,512]{1,0:T(8,128)(2,1)S(1)}, bf16[96,512]{1,0:T(8,128)(2,1)}, u32[]{:S(2)}) copy-start(bf16[96,512]{1,0:T(8,128)(2,1)} %param.33) | copy-start | bytes 294916
  27.6 20.8 %copy-start.17 = (f32[512]{0:T(512)S(1)}, f32[512]{0:T(512)}, u32[]{:S(2)}) copy-start(f32[512]{0:T(512)} %param.34) | copy-start | bytes 6148
  48.6 0.6 copy-start.10
  55.1 4.7 %copy-start.1 = (f32[24,64,8,64]{3,2,1,0:T(8,128)S(1)}, f32[24,64,8,64]{3,2,1,0:T(8,128)}, u32[]{:S(2)}) copy-start(f32[24,64,8,64]{3,2,1,0:T(8,128)} %reshape.195) | copy-start | bytes 9437188
  59.8 5.8 %copy-start.2 = (f32[24,64,8]{2,1,0:T(8,128)}, f32[24,64,8]{2,1,0:T(8,128)S(1)}, u32[]{:S(2)}) copy-start(f32[24,64,8]{2,1,0:T(8,128)S(1)} %multiply_reduce_fusion.1) | copy-start | bytes 147460
  65.6 9.1 %copy-start.12 = (bf16[24,512]{1,0:T(8,128)(2,1)S(1)}, bf16[24,512]{1,0:T(8,128)(2,1)}, u32[]{:S(2)}) copy-start(bf16[24,512]{1,0:T(8,128)(2,1)} %param.26) | copy-start | bytes 73732
  65.6 18.5 %copy-start.14 = (f32[2048]{0:T(1024)S(1)}, f32[2048]{0:T(1024)}, u32[]{:S(2)}) copy-start(f32[2048]{0:T(1024)} %convert_element_type.149) | copy-start | bytes 24580
  76.6 7.5 %copy-start.7 = (bf16[24,512]{1,0:T(8,128)(2,1)}, bf16[24,512]{1,0:T(8,128)(2,1)S(1)}, u32[]{:S(2)}) copy-start(bf16[24,512]{1,0:T(8,128)(2,1)S(1)} %fusion.28) | copy-start | bytes 73732
  84.2 0.6 copy-start.4
  114.0 0.9 copy-start.3
  117.9 4.2 %copy-start.5 = (bf16[24,2048]{1,0:T(8,128)(2,1)S(1)}, bf16[24,2048]{1,0:T(8,128)(2,1)}, u32[]{:S(2)}) copy-start(bf16[24,2048]{1,0:T(8,128)(2,1)} %copy-done.4) | copy-start | bytes 294916
  117.9 4.2 %copy-start.6 = (bf16[2048,128]{1,0:T(8,128)(2,1)S(1)}, bf16[2048,128]{1,0:T(8,128)(2,1)}, u32[]{:S(2)}) copy-start(bf16[2048,128]{1,0:T(8,128)(2,1)} %param.48) | copy-start | bytes 1572868
  121.8 51.3 %reduce-scatter.5.cloned.1.call-start = ((), (), s32[]{:S(2)}) async-start(), calls=%async_computation.5 | async-start | bytes 122880 | tf_op jit(solution)/shard_map/reduce_scatter | solution.py:123
  144.5 6.3 %copy-start.9 = (f32[24,512]{1,0:T(8,128)S(1)}, f32[24,512]{1,0:T(8,128)}, u32[]{:S(2)}) copy-start(f32[24,512]{1,0:T(8,128)} %get-tuple-element.6) | copy-start | bytes 147460
  144.5 6.3 %copy-start.11 = (f32[24,512]{1,0:T(8,128)S(1)}, f32[24,512]{1,0:T(8,128)}, u32[]{:S(2)}) copy-start(f32[24,512]{1,0:T(8,128)} %copy-done.10) | copy-start | bytes 147460
  150.8 10.4 %copy-start.19 = (f32[96]{0:T(128)S(1)}, f32[96]{0:T(128)}, u32[]{:S(2)}) copy-start(f32[96]{0:T(128)} %copy-done.18) | copy-start | bytes 1156
  150.8 22.3 %copy-start.8 = (bf16[24,512]{1,0:T(8,128)(2,1)S(1)}, bf16[24,512]{1,0:T(8,128)(2,1)}, u32[]{:S(2)}) copy-start(bf16[24,512]{1,0:T(8,128)(2,1)} %copy-done.7) | copy-start | bytes 73732
  157.8 11.6 %all-to-all-start.1 = ((bf16[8,1,18,512]{3,2,1,0:T(8,128)(2,1)}), bf16[8,1,18,512]{3,2,1,0:T(8,128)(2,1)S(1)}, u32[]{:S(2)}, u32[]{:S(2)}) async-start(bf16[8,1,18,512]{3,2,1,0:T(8,128)(2,1)} %bitcast.114), calls=%async_computation.2 | async-start | bytes 393216 | tf_op jit(solution)/shard_map/all_to_all | solution.py:167
Sparse Core Ops, SparseCore 0:
  121.9 24.2 reduce-scatter.2
  149.0 24.0 reduce-scatter.4
where the time goes:
time: 183 us; the launch traced here: 181 us
  blocking collectives  66.8 us (37%)
  local copies, waits for them, and re-layouts  37.1 us (20%)
  other arithmetic  26.2 us (14%)
  matrix products  22.4 us (12%)
  between operations  14.4 us (8%)
  waiting for transfers between devices  10.8 us (6%)
  starting transfers between devices  3.65 us (2%)
    all_to_all x1, blocking collectives, local(): lax.all_to_all(outgoing, 'ep', split_axis=0, concat_axis=0, tiled=True)  25.8 us
    dot_general x12, matrix products, product(): return jnp.dot(left, right, preferred_element_type=jnp.float32)  15.4 us
    psum x1, blocking collectives, local(): lax.psum((product(first_own, decay_down), product(first_own, iclr_down)),...  15.2 us
    mul x2, local copies, waits for them, and re-layouts, local(): recall[..., None] * scaled_removal[:, None]  11.6 us
    mul x3, local copies, waits for them, and re-layouts, local(): value_cols[..., None] * written[:, None]  10.1 us
    all_gather x1, blocking collectives, first_norm_rows(): gathered = lax.all_gather(token_rows, 'tp', axis=1, tiled=True)  10 us
    all_gather x1, blocking collectives, local(): heads_all = lax.all_gather(head_out, 'tp', axis=1, tiled=True)  8.39 us
    all_to_all x1, waiting for transfers between devices, local(): lax.all_to_all(summed, 'ep', split_axis=0, concat_axis=0, tiled=True)  8.19 us
  transfers between devices with their start and end apart: 3, of which 2 were waited for; matrix products, arithmetic and copies ran while one was open for 20% of the time, Pallas kernels for 0%

commit v1 on v0

v1 whole, which is shorter than its diff:
```python
import functools

import jax
import jax.numpy as jnp
from jax import lax
from jax.experimental import pallas as pl
from jax.experimental.pallas import tpu as pltpu
from jax.sharding import PartitionSpec as P

HEAD = 64
CORES = 2
GROUP = 8
norm_eps = 1e-06
head_eps = 0.00064
key_eps = 1e-06
F32 = jnp.float32
BF16 = jnp.bfloat16


def product(left, right):
    return jnp.dot(left, right, preferred_element_type=F32)


def kernel(
    tp, ep,
    x_ref, gains, vecs, routes, rweights,
    state_h, wr_h, wk_h, wv_h, dd_h, id_h, du_h, iu_h, wo_h, eg_h, eu_h, ed_h, dg_h, dup_h, ddn_h,
    out_ref, ns_h,
    st, wr, wk, wv, dd, idn, du, iu, wo, eg, eu, ed, dg, dup, ddn,
    xg, pbuf, pg, wbuf, wg, hbuf, hg, rbuf, grid, dbuf, drecv,
    rem_s, dr_s, val_s, dec_s, srem_s, wri_s, rec_s, q_s, rb,
    norm_s, mine_s, psend, precv, hsum, hrecv, qbuf, qrecv,
    lsem, ssem, rsem,
):
    nz = ep // CORES
    t = lax.axis_index("tp")
    e = lax.axis_index("ep")
    z = e // CORES
    core = lax.rem(e, CORES)
    mate = 1 - core
    S, W = x_ref.shape
    D = W * tp
    L = dd.shape[1]

    loads = {}
    pairs = [("dd", dd_h, dd), ("id", id_h, idn), ("wr", wr_h, wr), ("wk", wk_h, wk), ("wv", wv_h, wv),
             ("du", du_h, du), ("iu", iu_h, iu), ("st", state_h, st), ("wo", wo_h, wo),
             ("dg", dg_h, dg), ("dup", dup_h, dup), ("ddn", ddn_h, ddn),
             ("eg", eg_h.at[0], eg), ("eu", eu_h.at[0], eu), ("ed", ed_h.at[0], ed)]
    for i, (name, src, dst) in enumerate(pairs):
        loads[name] = pltpu.make_async_copy(src, dst, lsem.at[i])
        loads[name].start()
    next_copy = pltpu.make_async_copy(st, ns_h, lsem.at[len(pairs)])

    barrier = pltpu.get_barrier_semaphore()
    for d in range(1, tp):
        pl.semaphore_signal(barrier, inc=1, device_id={"ep": e, "tp": lax.rem(t + d, tp)},
                            device_id_type=pl.DeviceIdType.MESH)
    for d in range(1, ep):
        pl.semaphore_signal(barrier, inc=1, device_id={"ep": lax.rem(e + d, ep), "tp": t},
                            device_id_type=pl.DeviceIdType.MESH)
    pl.semaphore_wait(barrier, tp - 1 + ep - 1)

    sent = []

    def send(src, dst, dev_e, dev_t):
        i = len(sent)
        c = pltpu.make_async_remote_copy(
            src_ref=src, dst_ref=dst, send_sem=ssem.at[i], recv_sem=rsem.at[i],
            device_id={"ep": dev_e, "tp": dev_t}, device_id_type=pl.DeviceIdType.MESH)
        c.start()
        sent.append(c)
        return c

    def to_tp(src, dst):
        return [send(src, dst, e, lax.rem(t + d, tp)) for d in range(1, tp)]

    def all_cols(block):
        return jnp.concatenate([block(k) for k in range(tp)], axis=-1)

    xc = to_tp(x_ref, xg.at[t])
    xg[t] = x_ref[...]

    lane = lax.broadcasted_iota(jnp.int32, (S, 128), 1)
    wmat = jnp.zeros((S, 128), F32)
    for k in range(routes.shape[1]):
        wmat += jnp.where(lane == routes[:, k:k + 1], rweights[:, k:k + 1], 0.0)
    wbuf[...] = wmat
    wg[e] = wmat
    wc = [send(wbuf, wg.at[e], lax.rem(e + d, ep), t) for d in range(1, ep)]

    own = pl.ds(pl.multiple_of(t * W, 128), W)
    x_own = x_ref[...].astype(F32)
    xs = (x_own * gains[0:1, own]).astype(BF16)
    loads["dd"].wait()
    loads["id"].wait()
    pbuf[:, :L] = product(xs, dd[...])
    pbuf[:, 128:128 + L] = product(xs, idn[...])
    pg[t] = pbuf[...]
    pc = to_tp(pbuf, pg.at[t])

    C = min(256, W)
    ri = lax.broadcasted_iota(jnp.int32, (C, C), 0) // HEAD
    ci = lax.broadcasted_iota(jnp.int32, (C, C), 1) // HEAD
    ones = (ri == ci).astype(F32).astype(BF16)

    def seg(v):
        hi = v.astype(BF16)
        lo = (v - hi.astype(F32)).astype(BF16)
        return jnp.concatenate(
            [product(hi[:, c:c + C], ones) + product(lo[:, c:c + C], ones) for c in range(0, W, C)], axis=1)

    for c in xc:
        c.wait_recv()
    full = all_cols(lambda k: xg[k].astype(F32))
    inv = lax.rsqrt(jnp.mean(full * full, axis=1, keepdims=True) + norm_eps)
    first = (full * inv * gains[0:1, :]).astype(BF16)
    loads["wk"].wait()
    key = product(first, wk[...]).astype(BF16).astype(F32)
    loads["wr"].wait()
    recept = product(first, wr[...]).astype(BF16).astype(F32)
    loads["wv"].wait()
    value = product(first, wv[...]).astype(BF16).astype(F32)
    for c in pc:
        c.wait_recv()
    low = pg[0]
    for k in range(1, tp):
        low += pg[k]
    low = low * inv
    loads["du"].wait()
    loads["iu"].wait()
    decay_pre = vecs[0:1, :] + product(jnp.tanh(low[:, :L]).astype(BF16), du[...])
    decay = jnp.exp(-0.6065306597126334 * jax.nn.sigmoid(decay_pre))
    rate = jax.nn.sigmoid(vecs[1:2, :] + product(low[:, 128:128 + L].astype(BF16), iu[...]))
    scaled = key * vecs[2:3, :]
    removal = scaled * lax.rsqrt(seg(scaled * scaled) + key_eps)
    written = key * (1.0 + (rate - 1.0) * vecs[3:4, :])
    srem = removal * rate
    rem_s[...] = removal
    dr_s[...] = decay * recept
    val_s[...] = value
    dec_s[...] = decay
    srem_s[...] = srem
    wri_s[...] = written
    bonus_a = seg(srem * recept)
    bonus_b = seg(written * recept)

    eye = (lax.broadcasted_iota(jnp.int32, (HEAD, C), 0)
           == lax.rem(lax.broadcasted_iota(jnp.int32, (HEAD, C), 1), HEAD)).astype(F32)
    loads["st"].wait()

    def read_group(g, carry):
        for c in range(0, W, C):
            cols = slice(c, c + C)
            parts = []
            for k in range(GROUP):
                s = g * GROUP + k
                parts.append((st[s, :, cols] * rem_s[pl.ds(s, 1), cols]).astype(BF16))
            for k in range(GROUP):
                s = g * GROUP + k
                parts.append((st[s, :, cols] * dr_s[pl.ds(s, 1), cols]).astype(BF16))
            both = product(jnp.concatenate(parts, axis=0), ones)
            for k in range(GROUP):
                s = g * GROUP + k
                a = both[k * HEAD:(k + 1) * HEAD]
                rb[s, :, cols] = a
                rec_s[pl.ds(s, 1), cols] = jnp.sum(a * eye, axis=0, keepdims=True)
                b = both[(GROUP + k) * HEAD:(GROUP + k + 1) * HEAD]
                q_s[pl.ds(s, 1), cols] = jnp.sum(b * eye, axis=0, keepdims=True)
        return carry

    lax.fori_loop(0, S // GROUP, read_group, 0)
    read = q_s[...] - rec_s[...] * bonus_a + value * bonus_b
    cent = read - seg(read) * (1.0 / HEAD)
    var = seg(cent * cent) * (1.0 / HEAD)
    head = (cent * lax.rsqrt(var + head_eps) * vecs[4:5, :]).astype(BF16)
    hbuf[...] = head
    hg[t] = head
    hc = to_tp(hbuf, hg.at[t])

    def next_group(g, carry):
        for c in range(0, W, C):
            cols = slice(c, c + C)
            parts = []
            for k in range(GROUP):
                s = g * GROUP + k
                parts.append((eye * val_s[pl.ds(s, 1), cols]).astype(BF16))
            vals = product(jnp.concatenate(parts, axis=0), ones)
            for k in range(GROUP):
                s = g * GROUP + k
                st[s, :, cols] = (st[s, :, cols] * dec_s[pl.ds(s, 1), cols]
                                  - rb[s, :, cols] * srem_s[pl.ds(s, 1), cols]
                                  + vals[k * HEAD:(k + 1) * HEAD] * wri_s[pl.ds(s, 1), cols])
        return carry

    lax.fori_loop(0, S // GROUP, next_group, 0)
    next_copy.start()

    for c in hc:
        c.wait_recv()
    loads["wo"].wait()
    mixer = product(all_cols(lambda k: hg[k]), wo[...]).astype(BF16)
    residual = (x_own + mixer.astype(F32)).astype(BF16)
    rbuf[...] = residual
    grid[core, z, t] = residual

    tc = to_tp(rbuf, grid.at[core, z, t])
    zc = [send(rbuf, grid.at[core, z, t], lax.rem(z + d, nz) * CORES + core, t) for d in range(1, nz)]
    fc = []
    for d in range(1, nz):
        zc[d - 1].wait_recv()
        zz = lax.rem(z - d + nz, nz)
        fc.append(to_tp(grid.at[core, zz, t], grid.at[core, zz, t]))
    for c in tc:
        c.wait_recv()
    mc = [send(grid.at[core, z], grid.at[core, z], z * CORES + mate, t)]

    def normed(rows):
        scale = lax.rsqrt(jnp.mean(rows * rows, axis=-1, keepdims=True) + norm_eps)
        return rows * scale * gains[1:2, :]

    second = normed(all_cols(lambda k: grid[core, z, k].astype(F32))).astype(BF16)
    for n in ("dg", "dup", "ddn"):
        loads[n].wait()
    dhid = (jax.nn.silu(product(second, dg[...])) * product(second, dup[...])).astype(BF16)
    dpart = product(dhid, ddn[...])
    for k in range(tp):
        dbuf[k] = dpart[:, k * W:(k + 1) * W].astype(BF16)
    dc = [send(dbuf.at[lax.rem(t + d, tp)], drecv.at[d - 1], e, lax.rem(t + d, tp)) for d in range(1, tp)]
    mix = jax.nn.sigmoid(jnp.sum(second.astype(F32) * gains[2:3, :], axis=1, keepdims=True))

    for d in range(1, nz):
        for c in fc[d - 1]:
            c.wait_recv()
        zz = lax.rem(z - d + nz, nz)
        mc.append(send(grid.at[core, zz], grid.at[core, zz], z * CORES + mate, t))
    for c in mc:
        c.wait_recv()
    for k in range(nz):
        rows = jnp.concatenate(
            [all_cols(lambda j, i=i: grid[i, k, j].astype(F32)) for i in range(CORES)], axis=0)
        norm_s[k * CORES * S:(k + 1) * CORES * S, :] = normed(rows).astype(BF16)

    for c in wc:
        c.wait_recv()
    wall = wg[...].reshape(ep * S, 128)
    wcol = jnp.sum(jnp.where(lax.broadcasted_iota(jnp.int32, (ep * S, 128), 1) == e, wall, 0.0),
                   axis=1, keepdims=True)
    loads["eg"].wait()
    gate = product(norm_s[...], eg[...])
    loads["eu"].wait()
    hidden = (jax.nn.silu(gate) * product(norm_s[...], eu[...])).astype(BF16)
    loads["ed"].wait()
    upper = core.astype(F32)
    order = list(range(1, tp)) + [0]
    rc = []
    for d in order:
        c = lax.rem(t + d, tp)
        part = product(hidden, ed[:, pl.ds(pl.multiple_of(c * W, 128), W)]) * wcol
        part = part.reshape(nz, CORES, S, W)
        psend[d] = (part[:, 0] * upper + part[:, 1] * (1.0 - upper)).astype(BF16)
        mine_s[d] = part[:, 1] * upper + part[:, 0] * (1.0 - upper)
        rc.append(send(psend.at[d], precv.at[d], z * CORES + mate, t))
    sc = []
    for i, d in enumerate(order):
        rc[i].wait_recv()
        both = mine_s[d] + precv[d].astype(F32)
        if d:
            hsum[d - 1] = both.astype(BF16)
            sc.append(send(hsum.at[d - 1], hrecv.at[d - 1], e, lax.rem(t + d, tp)))
        else:
            total = both
    for d in range(1, tp):
        sc[d - 1].wait_recv()
        total += hrecv[d - 1].astype(F32)
    qbuf[...] = total.astype(BF16)
    qc = [send(qbuf.at[lax.rem(z + d, nz)], qrecv.at[d - 1], lax.rem(z + d, nz) * CORES + core, t)
          for d in range(1, nz)]
    for c in dc:
        c.wait_recv()
    dense = dbuf[t].astype(F32)
    for d in range(1, tp):
        dense += drecv[d - 1].astype(F32)
    acc = residual.astype(F32) + mix * dense + qbuf[z].astype(F32)
    for d in range(1, nz):
        qc[d - 1].wait_recv()
        acc += qrecv[d - 1].astype(F32)
    out_ref[...] = acc.astype(BF16)
    next_copy.wait()
    for c in sent:
        c.wait_send()


def local(
    tp, ep, token_rows, prior_state, first_gain, w_recept, w_key, w_value, decay_down, decay_up, decay_base,
    iclr_down, iclr_up, iclr_base, key_scale, key_mix, head_gain, w_out, second_gain, routes, route_weights,
    exp_gate, exp_up, exp_down, dense_gate, dense_up, dense_down, dense_mix,
):
    S, W = token_rows.shape
    D = W * tp
    nz = ep // CORES
    gains = jnp.stack([first_gain, second_gain, dense_mix]).astype(F32)
    vecs = jnp.stack([decay_base, iclr_base, key_scale.astype(F32), key_mix.astype(F32), head_gain.astype(F32)])
    big = [prior_state, w_recept, w_key, w_value, decay_down, iclr_down, decay_up, iclr_up, w_out,
           exp_gate, exp_up, exp_down, dense_gate, dense_up, dense_down]
    V = lambda a: pltpu.VMEM(a.shape, a.dtype)
    E = lambda a: pltpu.VMEM(a.shape[1:], a.dtype)
    copies = (4 * (tp - 1) + (ep - 1) + 2 * (nz - 1) + (nz - 1) * (tp - 1) + nz + 2 * (tp - 1) + tp)
    row = pltpu.VMEM((S, W), F32)
    scratch = [
        V(prior_state), V(w_recept), V(w_key), V(w_value), V(decay_down), V(iclr_down), V(decay_up), V(iclr_up),
        V(w_out), E(exp_gate), E(exp_up), E(exp_down), V(dense_gate), V(dense_up), V(dense_down),
        pltpu.VMEM((tp, S, W), BF16), pltpu.VMEM((S, 256), F32), pltpu.VMEM((tp, S, 256), F32),
        pltpu.VMEM((S, 128), F32), pltpu.VMEM((ep, S, 128), F32),
        pltpu.VMEM((S, W), BF16), pltpu.VMEM((tp, S, W), BF16), pltpu.VMEM((S, W), BF16),
        pltpu.VMEM((CORES, nz, tp, S, W), BF16), pltpu.VMEM((tp, S, W), BF16), pltpu.VMEM((tp - 1, S, W), BF16),
        row, row, row, row, row, row, row, row, V(prior_state),
        pltpu.VMEM((ep * S, D), BF16), pltpu.VMEM((tp, nz, S, W), F32), pltpu.VMEM((tp, nz, S, W), BF16),
        pltpu.VMEM((tp, nz, S, W), BF16), pltpu.VMEM((tp - 1, nz, S, W), BF16),
        pltpu.VMEM((tp - 1, nz, S, W), BF16), pltpu.VMEM((nz, S, W), BF16), pltpu.VMEM((nz - 1, S, W), BF16),
        pltpu.SemaphoreType.DMA((len(big) + 1,)), pltpu.SemaphoreType.DMA((copies,)),
        pltpu.SemaphoreType.DMA((copies,)),
    ]
    vm = pl.BlockSpec(memory_space=pltpu.VMEM)
    anym = pl.BlockSpec(memory_space=pl.ANY)
    return pl.pallas_call(
        functools.partial(kernel, tp, ep),
        name="layer",
        out_shape=(jax.ShapeDtypeStruct((S, W), BF16), jax.ShapeDtypeStruct(prior_state.shape, F32)),
        in_specs=[vm] * 5 + [anym] * len(big),
        out_specs=(vm, anym),
        scratch_shapes=scratch,
        compiler_params=pltpu.CompilerParams(
            collective_id=0, has_side_effects=True, vmem_limit_bytes=63 * 1024 * 1024),
    )(token_rows, gains, vecs, routes, route_weights, *big)


def solution(mesh):
    in_specs = (
        P("ep", "tp"), P("ep", None, "tp"), P(), P(None, "tp"), P(None, "tp"), P(None, "tp"), P("tp", None),
        P(None, "tp"), P("tp"), P("tp", None), P(None, "tp"), P("tp"), P("tp"), P("tp"), P("tp"), P(None, "tp"),
        P(), P("ep", None), P("ep", None), P("ep", None, "tp"), P("ep", None, "tp"), P("ep", "tp", None),
        P(None, "tp"), P(None, "tp"), P("tp", None), P(),
    )
    out_specs = (P("ep", "tp"), P("ep", None, "tp"))
    body = functools.partial(local, mesh.shape["tp"], mesh.shape["ep"])
    return jax.shard_map(body, mesh=mesh, in_specs=in_specs, out_specs=out_specs, check_vma=False)
```

time: 183 us -> 60.1 us (0.33)
  blocking collectives: 66.8 us -> 0 us
  Pallas kernels: 0 us -> 41.5 us
  other arithmetic: 26.2 us -> 2.69 us
  matrix products: 22.4 us -> 0 us
  local copies, waits for them, and re-layouts: 37.1 us -> 14.8 us
  between operations: 14.4 us -> 0.64 us
  waiting for transfers between devices: 10.8 us -> 0 us
  starting transfers between devices: 3.65 us -> 0 us
    pallas_call x0 -> x1, Pallas kernels: none -> 41.5 us  [local(): pl.pallas_call(functools.partial(kernel, tp, ep), name='layer', out_shape...]
    all_to_all x1 -> x0, blocking collectives: 25.8 us -> none  [local(): lax.all_to_all(outgoing, 'ep', split_axis=0, concat_axis=0, tiled=True)]
    all_gather x3 -> x0, blocking collectives: 25.7 us -> none  [the longest x1 10 us: first_norm_rows(): gathered = lax.all_gather(token_rows, 'tp', axis=1, tiled=True)]
    mul x13 -> x0, local copies, waits for them, and re-layouts: 23.1 us -> none  [the longest x2 11.6 us: local(): recall[..., None] * scaled_removal[:, None]]
    dot_general x15 -> x0, matrix products: 22.4 us -> none  [the longest x12 15.4 us: product(): return jnp.dot(left, right, preferred_element_type=jnp.float32)]
    psum x1 -> x0, blocking collectives: 15.2 us -> none  [local(): lax.psum((product(first_own, decay_down), product(first_own, iclr_down)),...]
    reduce_sum x8 -> x0, other arithmetic: 11.2 us -> none  [the longest x1 5.77 us: local(): jnp.sum(state_grid * recept.astype(jnp.float32).reshape(seq_count, 1, hea...]
    all_to_all x1 -> x0, waiting for transfers between devices: 8.19 us -> none  [local(): lax.all_to_all(summed, 'ep', split_axis=0, concat_axis=0, tiled=True)]
  transfers between devices with their start and end apart: 3 -> 0, of which waited for: 2 -> 0; matrix products, arithmetic and copies ran while one was open for 20% -> 0% of each run, Pallas kernels for 0% -> 0%
where the time goes in v1:
time: 60.1 us; the launch traced here: 59.6 us
  Pallas kernels  41.5 us (69%)
  local copies, waits for them, and re-layouts  14.8 us (25%)
  other arithmetic  2.69 us (4%)
  between operations  0.64 us (1%)
    pallas_call x1, Pallas kernels, local(): pl.pallas_call(functools.partial(kernel, tp, ep), name='layer', out_shape...  41.5 us
    unnamed x6, local copies, waits for them, and re-layouts  11.4 us
    another operation x3, local copies, waits for them, and re-layouts, local(): gains = jnp.stack([first_gain, second_gain, dense_mix]).astype(F32)  2.08 us
    another operation x3, other arithmetic, local(): jnp.stack([decay_base, iclr_base, key_scale.astype(F32), key_mix.astype(F...  2.04 us
    another operation x1, local copies, waits for them, and re-layouts, local(): jnp.stack([decay_base, iclr_base, key_scale.astype(F32), key_mix.astype(F...  1.32 us

profile of v1, /device:TPU:0, one launch (start us, length us, event | category | flops | bytes accessed | tf_op | source)
XLA Modules:
  0.0 59.6 jit_solution(8579677350725619908)
XLA Ops:
  0.6 0.7 %stack.52 = f32[512]{0:T(512)S(1)} convert(bf16[512]{0:T(512)(128)(2,1)} %param.38) | non-fusion elementwise | flops 512 | bytes 3072 | tf_op jit(solution)/shard_map/stack | solution.py:303
  1.3 0.7 %stack.53 = f32[512]{0:T(512)S(1)} convert(bf16[512]{0:T(512)(128)(2,1)} %param.39) | non-fusion elementwise | flops 512 | bytes 3072 | tf_op jit(solution)/shard_map/stack | solution.py:303
  2.0 0.7 %stack.54 = f32[512]{0:T(512)S(1)} convert(bf16[512]{0:T(512)(128)(2,1)} %param.40) | non-fusion elementwise | flops 512 | bytes 3072 | tf_op jit(solution)/shard_map/stack | solution.py:303
  2.7 0.7 %stack.39 = bf16[1,2048]{1,0:T(2,128)(2,1)S(1)} reshape(bf16[2048]{0:T(1024)(128)(2,1)} %param.28) | data formatting | bytes 8192 | tf_op jit(solution)/shard_map/stack | solution.py:302
  3.4 0.7 %stack.40 = bf16[1,2048]{1,0:T(2,128)(2,1)S(1)} reshape(bf16[2048]{0:T(1024)(128)(2,1)} %param.42) | data formatting | bytes 8192 | tf_op jit(solution)/shard_map/stack | solution.py:302
  4.1 0.7 %stack.41 = bf16[1,2048]{1,0:T(2,128)(2,1)S(1)} reshape(bf16[2048]{0:T(1024)(128)(2,1)} %param.51) | data formatting | bytes 8192 | tf_op jit(solution)/shard_map/stack | solution.py:302
  4.8 0.6 %maximum_convert_fusion.gains = f32[3,2048]{1,0:T(4,128)} fusion(bf16[1,2048]{1,0:T(2,128)(2,1)S(1)} %stack.41, bf16[1,2048]{1,0:T(2,128)(2,1)S(1)} %stack.40, bf16[1,2048]{1,0:T(2,128)(2,1)S(1)} %stack.39), kind=kLoop, calls=%fused_computation | loop fusion | flops 36864 | bytes 36864 | tf_op jit(solution)/shard_map/convert_element_type | solution.py:302
  5.4 1.3 %stack.51.vecs = f32[5,512]{1,0:T(8,128)} concatenate(f32[1,512]{1,0:T(1,128)} %bitcast.8, f32[1,512]{1,0:T(1,128)} %bitcast.9, f32[1,512]{1,0:T(1,128)S(1)} %bitcast.5, f32[1,512]{1,0:T(1,128)S(1)} %bitcast.6, f32[1,512]{1,0:T(1,128)S(1)} %bitcast.7), dimensions={0} | concatenate | bytes 20480 | tf_op jit(solution)/shard_map/stack | solution.py:303
  6.7 1.4 %copy.28.routes = s32[24,4]{1,0:T(8,128)} copy(s32[24,4]{0,1:T(4,128)} %param.43) | data formatting | bytes 768 | tf_op args[17]
  8.1 1.4 %copy.29.rweights = f32[24,4]{1,0:T(8,128)} copy(f32[24,4]{0,1:T(4,128)} %param.44) | data formatting | bytes 768 | tf_op args[18]
  9.4 1.7 %copy.30.dd_h = bf16[512,96]{1,0:T(8,128)(2,1)} copy(bf16[512,96]{0,1:T(8,128)(2,1)} %param.32) | data formatting | bytes 196608 | tf_op args[6]
  11.1 1.6 %copy.31.id_h = bf16[512,96]{1,0:T(8,128)(2,1)} copy(bf16[512,96]{0,1:T(8,128)(2,1)} %param.35) | data formatting | bytes 196608 | tf_op args[9]
  12.7 41.5 %layer.1 = (bf16[24,512]{1,0:T(8,128)(2,1)}, f32[24,64,512]{2,1,0:T(8,128)}) custom-call(bf16[24,512]{1,0:T(8,128)(2,1)} %x_ref.1, f32[3,2048]{1,0:T(4,128)} %maximum_convert_fusion.gains, f32[5,512]{1,0:T(8,128)} %stack.51.vecs, s32[24,4]{1,0:T(8,128)} %copy.28.routes, f32[24,4]{1,0:T(8,128)} %copy.29.rweights, f32[24,64,512]{2,1,0:T(8,128)} %state_h.1, ...), custom_call_target="tpu_custom_call" | custom-call | tf_op jit(solution)/shard_map/layer/pallas_call | solution.py:326
  54.2 1.3 %copy.34 = bf16[24,512]{1,0:T(8,128)(2,1)} copy(bf16[24,512]{1,0:T(8,128)(2,1)} %get-tuple-element.4) | data formatting | bytes 49152
  55.5 4.0 %copy.35 = f32[24,64,512]{2,1,0:T(8,128)} copy(f32[24,64,512]{2,1,0:T(8,128)} %get-tuple-element.5) | data formatting | bytes 6291456

commit v2 on v1

--- a/solution.py
+++ b/solution.py
@@ -10,6 +10,7 @@
 HEAD = 64
 CORES = 2
 GROUP = 8
+VMEM_BYTES = 67043328
 norm_eps = 1e-06
 head_eps = 0.00064
 key_eps = 1e-06
@@ -21,9 +22,13 @@
     return jnp.dot(left, right, preferred_element_type=F32)
 
 
+def product_t(left, right):
+    return lax.dot_general(left, right, (((1,), (1,)), ((), ())), preferred_element_type=F32)
+
+
 def kernel(
     tp, ep,
-    x_ref, gains, vecs, routes, rweights,
+    x_ref, fg_ref, sg_ref, dm_ref, db_ref, ib_ref, ks_ref, km_ref, hgain_ref, routes, rweights,
     state_h, wr_h, wk_h, wv_h, dd_h, id_h, du_h, iu_h, wo_h, eg_h, eu_h, ed_h, dg_h, dup_h, ddn_h,
     out_ref, ns_h,
     st, wr, wk, wv, dd, idn, du, iu, wo, eg, eu, ed, dg, dup, ddn,
@@ -40,7 +45,10 @@
     mate = 1 - core
     S, W = x_ref.shape
     D = W * tp
-    L = dd.shape[1]
+    L = dd.shape[0]
+
+    def line(ref):
+        return ref[...].astype(F32).reshape(1, -1)
 
     loads = {}
     pairs = [("dd", dd_h, dd), ("id", id_h, idn), ("wr", wr_h, wr), ("wk", wk_h, wk), ("wv", wv_h, wv),
@@ -50,7 +58,6 @@
     for i, (name, src, dst) in enumerate(pairs):
         loads[name] = pltpu.make_async_copy(src, dst, lsem.at[i])
         loads[name].start()
-    next_copy = pltpu.make_async_copy(st, ns_h, lsem.at[len(pairs)])
 
     barrier = pltpu.get_barrier_semaphore()
     for d in range(1, tp):
@@ -81,21 +88,28 @@
     xc = to_tp(x_ref, xg.at[t])
     xg[t] = x_ref[...]
 
-    lane = lax.broadcasted_iota(jnp.int32, (S, 128), 1)
-    wmat = jnp.zeros((S, 128), F32)
-    for k in range(routes.shape[1]):
-        wmat += jnp.where(lane == routes[:, k:k + 1], rweights[:, k:k + 1], 0.0)
+    expert = lax.broadcasted_iota(jnp.int32, (128, S), 0)
+    wide = jnp.zeros((128, S), F32)
+    for k in range(routes.shape[0]):
+        wide += jnp.where(expert == routes[k:k + 1, :], rweights[k:k + 1, :], 0.0)
+    same = (lax.broadcasted_iota(jnp.int32, (S, S), 0) == lax.broadcasted_iota(jnp.int32, (S, S), 1)).astype(F32)
+    wmat = lax.dot_general(same, wide, (((1,), (1,)), ((), ())), precision=lax.Precision.HIGHEST,
+                           preferred_element_type=F32)
     wbuf[...] = wmat
     wg[e] = wmat
     wc = [send(wbuf, wg.at[e], lax.rem(e + d, ep), t) for d in range(1, ep)]
 
     own = pl.ds(pl.multiple_of(t * W, 128), W)
     x_own = x_ref[...].astype(F32)
-    xs = (x_own * gains[0:1, own]).astype(BF16)
+    first_gain = line(fg_ref)
+    own_gain = first_gain[:, :W]
+    for k in range(1, tp):
+        own_gain = jnp.where(t == k, first_gain[:, k * W:(k + 1) * W], own_gain)
+    xs = (x_own * own_gain).astype(BF16)
     loads["dd"].wait()
     loads["id"].wait()
-    pbuf[:, :L] = product(xs, dd[...])
-    pbuf[:, 128:128 + L] = product(xs, idn[...])
+    pbuf[:, :L] = product_t(xs, dd[...])
+    pbuf[:, 128:128 + L] = product_t(xs, idn[...])
     pg[t] = pbuf[...]
     pc = to_tp(pbuf, pg.at[t])
 
@@ -114,7 +128,7 @@
         c.wait_recv()
     full = all_cols(lambda k: xg[k].astype(F32))
     inv = lax.rsqrt(jnp.mean(full * full, axis=1, keepdims=True) + norm_eps)
-    first = (full * inv * gains[0:1, :]).astype(BF16)
+    first = (full * inv * first_gain).astype(BF16)
     loads["wk"].wait()
     key = product(first, wk[...]).astype(BF16).astype(F32)
     loads["wr"].wait()
@@ -129,12 +143,12 @@
     low = low * inv
     loads["du"].wait()
     loads["iu"].wait()
-    decay_pre = vecs[0:1, :] + product(jnp.tanh(low[:, :L]).astype(BF16), du[...])
+    decay_pre = line(db_ref) + product(jnp.tanh(low[:, :L]).astype(BF16), du[...])
     decay = jnp.exp(-0.6065306597126334 * jax.nn.sigmoid(decay_pre))
-    rate = jax.nn.sigmoid(vecs[1:2, :] + product(low[:, 128:128 + L].astype(BF16), iu[...]))
-    scaled = key * vecs[2:3, :]
+    rate = jax.nn.sigmoid(line(ib_ref) + product(low[:, 128:128 + L].astype(BF16), iu[...]))
+    scaled = key * line(ks_ref)
     removal = scaled * lax.rsqrt(seg(scaled * scaled) + key_eps)
-    written = key * (1.0 + (rate - 1.0) * vecs[3:4, :])
+    written = key * (1.0 + (rate - 1.0) * line(km_ref))
     srem = removal * rate
     rem_s[...] = removal
     dr_s[...] = decay * recept
@@ -173,7 +187,7 @@
     read = q_s[...] - rec_s[...] * bonus_a + value * bonus_b
     cent = read - seg(read) * (1.0 / HEAD)
     var = seg(cent * cent) * (1.0 / HEAD)
-    head = (cent * lax.rsqrt(var + head_eps) * vecs[4:5, :]).astype(BF16)
+    head = (cent * lax.rsqrt(var + head_eps) * line(hgain_ref)).astype(BF16)
     hbuf[...] = head
     hg[t] = head
     hc = to_tp(hbuf, hg.at[t])
@@ -188,13 +202,12 @@
             vals = product(jnp.concatenate(parts, axis=0), ones)
             for k in range(GROUP):
                 s = g * GROUP + k
-                st[s, :, cols] = (st[s, :, cols] * dec_s[pl.ds(s, 1), cols]
+                ns_h[s, :, cols] = (st[s, :, cols] * dec_s[pl.ds(s, 1), cols]
                                   - rb[s, :, cols] * srem_s[pl.ds(s, 1), cols]
                                   + vals[k * HEAD:(k + 1) * HEAD] * wri_s[pl.ds(s, 1), cols])
         return carry
 
-    lax.fori_loop(0, S // GROUP, next_group, 0)
-    next_copy.start()
+    next_group(0, 0)
 
     for c in hc:
         c.wait_recv()
@@ -215,9 +228,11 @@
         c.wait_recv()
     mc = [send(grid.at[core, z], grid.at[core, z], z * CORES + mate, t)]
 
+    second_gain = line(sg_ref)
+
     def normed(rows):
         scale = lax.rsqrt(jnp.mean(rows * rows, axis=-1, keepdims=True) + norm_eps)
-        return rows * scale * gains[1:2, :]
+        return rows * scale * second_gain
 
     second = normed(all_cols(lambda k: grid[core, z, k].astype(F32))).astype(BF16)
     for n in ("dg", "dup", "ddn"):
@@ -227,19 +242,19 @@
     for k in range(tp):
         dbuf[k] = dpart[:, k * W:(k + 1) * W].astype(BF16)
     dc = [send(dbuf.at[lax.rem(t + d, tp)], drecv.at[d - 1], e, lax.rem(t + d, tp)) for d in range(1, tp)]
-    mix = jax.nn.sigmoid(jnp.sum(second.astype(F32) * gains[2:3, :], axis=1, keepdims=True))
+    mix = jax.nn.sigmoid(jnp.sum(second.astype(F32) * line(dm_ref), axis=1, keepdims=True))
 
     for d in range(1, nz):
         for c in fc[d - 1]:
             c.wait_recv()
         zz = lax.rem(z - d + nz, nz)
         mc.append(send(grid.at[core, zz], grid.at[core, zz], z * CORES + mate, t))
-    for c in mc:
-        c.wait_recv()
-    for k in range(nz):
+    for d in range(nz):
+        mc[d].wait_recv()
+        zz = lax.rem(z - d + nz, nz)
         rows = jnp.concatenate(
-            [all_cols(lambda j, i=i: grid[i, k, j].astype(F32)) for i in range(CORES)], axis=0)
-        norm_s[k * CORES * S:(k + 1) * CORES * S, :] = normed(rows).astype(BF16)
+            [all_cols(lambda j, i=i: grid[i, zz, j].astype(F32)) for i in range(CORES)], axis=0)
+        norm_s[pl.ds(pl.multiple_of(zz * CORES * S, 16), CORES * S), :] = normed(rows).astype(BF16)
 
     for c in wc:
         c.wait_recv()
@@ -270,6 +285,7 @@
             sc.append(send(hsum.at[d - 1], hrecv.at[d - 1], e, lax.rem(t + d, tp)))
         else:
             total = both
+    lax.fori_loop(1, S // GROUP, next_group, 0)
     for d in range(1, tp):
         sc[d - 1].wait_recv()
         total += hrecv[d - 1].astype(F32)
@@ -286,7 +302,6 @@
         qc[d - 1].wait_recv()
         acc += qrecv[d - 1].astype(F32)
     out_ref[...] = acc.astype(BF16)
-    next_copy.wait()
     for c in sent:
         c.wait_send()
 
@@ -299,13 +314,15 @@
     S, W = token_rows.shape
     D = W * tp
     nz = ep // CORES
-    gains = jnp.stack([first_gain, second_gain, dense_mix]).astype(F32)
-    vecs = jnp.stack([decay_base, iclr_base, key_scale.astype(F32), key_mix.astype(F32), head_gain.astype(F32)])
+    decay_down, iclr_down = decay_down.T, iclr_down.T
+    small = [token_rows, first_gain, second_gain, dense_mix, decay_base, iclr_base, key_scale, key_mix, head_gain,
+             routes.T, route_weights.T]
     big = [prior_state, w_recept, w_key, w_value, decay_down, iclr_down, decay_up, iclr_up, w_out,
            exp_gate, exp_up, exp_down, dense_gate, dense_up, dense_down]
     V = lambda a: pltpu.VMEM(a.shape, a.dtype)
     E = lambda a: pltpu.VMEM(a.shape[1:], a.dtype)
     copies = (4 * (tp - 1) + (ep - 1) + 2 * (nz - 1) + (nz - 1) * (tp - 1) + nz + 2 * (tp - 1) + tp)
+    room = pl.cdiv(4 * prior_state.size + 2 * token_rows.size, 8192) * 8192
     row = pltpu.VMEM((S, W), F32)
     scratch = [
         V(prior_state), V(w_recept), V(w_key), V(w_value), V(decay_down), V(iclr_down), V(decay_up), V(iclr_up),
@@ -318,21 +335,21 @@
         pltpu.VMEM((ep * S, D), BF16), pltpu.VMEM((tp, nz, S, W), F32), pltpu.VMEM((tp, nz, S, W), BF16),
         pltpu.VMEM((tp, nz, S, W), BF16), pltpu.VMEM((tp - 1, nz, S, W), BF16),
         pltpu.VMEM((tp - 1, nz, S, W), BF16), pltpu.VMEM((nz, S, W), BF16), pltpu.VMEM((nz - 1, S, W), BF16),
-        pltpu.SemaphoreType.DMA((len(big) + 1,)), pltpu.SemaphoreType.DMA((copies,)),
+        pltpu.SemaphoreType.DMA((len(big),)), pltpu.SemaphoreType.DMA((copies,)),
         pltpu.SemaphoreType.DMA((copies,)),
     ]
     vm = pl.BlockSpec(memory_space=pltpu.VMEM)
-    anym = pl.BlockSpec(memory_space=pl.ANY)
+    anym = pl.BlockSpec(memory_space=pltpu.HBM)
     return pl.pallas_call(
         functools.partial(kernel, tp, ep),
         name="layer",
-        out_shape=(jax.ShapeDtypeStruct((S, W), BF16), jax.ShapeDtypeStruct(prior_state.shape, F32)),
-        in_specs=[vm] * 5 + [anym] * len(big),
-        out_specs=(vm, anym),
+        out_shape=(pltpu.VMEM((S, W), BF16), pltpu.VMEM(prior_state.shape, F32)),
+        in_specs=[vm] * len(small) + [anym] * len(big),
+        out_specs=(vm, vm),
         scratch_shapes=scratch,
         compiler_params=pltpu.CompilerParams(
-            collective_id=0, has_side_effects=True, vmem_limit_bytes=63 * 1024 * 1024),
-    )(token_rows, gains, vecs, routes, route_weights, *big)
+            collective_id=0, has_side_effects=True, vmem_limit_bytes=VMEM_BYTES - room),
+    )(*small, *big)
 
 
 def solution(mesh):

time: 60.1 us -> 43.9 us (0.73)
  local copies, waits for them, and re-layouts: 14.8 us -> 2.27 us
  other arithmetic: 2.69 us -> 0 us
  Pallas kernels: 41.5 us -> 40.8 us
    unnamed x6 -> x2, local copies, waits for them, and re-layouts: 11.4 us -> 2.27 us
    another operation x4 -> x0, local copies, waits for them, and re-layouts: 3.4 us -> none  [the longest x3 2.08 us: local(): gains = jnp.stack([first_gain, second_gain, dense_mix]).astype(F32)]
    another operation x3 -> x0, other arithmetic: 2.04 us -> none  [local(): jnp.stack([decay_base, iclr_base, key_scale.astype(F32), key_mix.astype(F...]
    convert_element_type x1 -> x0, other arithmetic: 0.65 us -> none  [local(): gains = jnp.stack([first_gain, second_gain, dense_mix]).astype(F32)]
    pallas_call x1, Pallas kernels: 41.5 us -> 40.8 us  [local(): pl.pallas_call(functools.partial(kernel, tp, ep), name='layer', out_shape...]
where the time goes in v2:
time: 43.9 us; the launch traced here: 43.8 us
  Pallas kernels  40.8 us (93%)
  local copies, waits for them, and re-layouts  2.27 us (5%)
  between operations  0.65 us (1%)
    pallas_call x1, Pallas kernels, local(): pl.pallas_call(functools.partial(kernel, tp, ep), name='layer', out_shape...  40.8 us
    unnamed x2, local copies, waits for them, and re-layouts  2.27 us

profile of v2, /device:TPU:0, one launch (start us, length us, event | category | flops | bytes accessed | tf_op | source)
XLA Modules:
  0.0 43.8 jit_solution(11763126743822175001)
XLA Ops:
  0.6 40.8 %layer.1 = (bf16[24,512]{1,0:T(8,128)(2,1)S(1)}, f32[24,64,512]{2,1,0:T(8,128)S(1)}) custom-call(bf16[24,512]{1,0:T(8,128)(2,1)} %x_ref.1, bf16[2048]{0:T(1024)(128)(2,1)} %fg_ref.1, bf16[2048]{0:T(1024)(128)(2,1)} %sg_ref.1, bf16[2048]{0:T(1024)(128)(2,1)} %dm_ref.1, f32[512]{0:T(512)} %db_ref.1, f32[512]{0:T(512)} %ib_ref.1, bf16[512]{0:T(512)(128)(2,1)} %ks_ref.1, ...), custom_call_target="tpu_custom_call" | custom-call | tf_op jit(solution)/shard_map/layer/pallas_call | solution.py:343
  41.5 0.6 %copy.30 = bf16[24,512]{1,0:T(8,128)(2,1)} copy(bf16[24,512]{1,0:T(8,128)(2,1)S(1)} %get-tuple-element.2) | data formatting | bytes 49152
  42.1 1.7 %copy.31 = f32[24,64,512]{2,1,0:T(8,128)} copy(f32[24,64,512]{2,1,0:T(8,128)S(1)} %get-tuple-element.3) | data formatting | bytes 6291456
